TPU v7x, 32 devices: a whole 2x2x4 slice. The times are simulated.
32 devices in a mesh: grp: 2 (over x), ep: 16 (over z, y, core).
Axes of the slice: x: 2, y: 2, z: 4, core: 2. Of those that a mesh axis runs over, the one named last changes fastest.
Arguments:
- stream: bfloat16 [8192, 2048], P(('grp', 'ep')), parts along dimension 0, may hold values from -6 to 6
- norm_gain: float32 [2048], replicated, may hold values from 0.1 to 1.9
- routing: int32 [8192, 4], P(('grp', 'ep')), parts along dimension 0, may hold values from 0 to 31, all different within a row; in each aligned block of 256 rows (0 to 255, 256 to 511, ...) at most 64 rows name the same one
- gates: float32 [8192, 4], P(('grp', 'ep')), parts along dimension 0, may hold values from 0.1 to 1
- w_gate: bfloat16 [32, 2048, 512], P('ep'), may hold values from -0.125 to 0.125
- w_up: bfloat16 [32, 2048, 512], P('ep'), may hold values from -0.125 to 0.125
- w_down: bfloat16 [32, 512, 2048], P('ep'), may hold values from -0.25 to 0.25
- shared_gate: bfloat16 [2048, 512], replicated, may hold values from -0.125 to 0.125
- shared_up: bfloat16 [2048, 512], replicated, may hold values from -0.125 to 0.125
- shared_down: bfloat16 [512, 2048], replicated, may hold values from -0.25 to 0.25
Outputs:
- mixed: bfloat16 [8192, 2048], P(('grp', 'ep')), parts along dimension 0
There are 2 independent parts, one for each index of `grp`. A program takes and returns all parts, laid end to end along the dimension named above; an argument that names none is the same for every part. Nothing has to cross between parts.
Inputs may be any that keep to these rules, and one draw needn't show every extreme that they name: `routing`: each token names 4 different experts. Among the 256 tokens of one index of ep no expert is named more than 64 times, and on some index an expert is named exactly 64 times.
All inputs are finite; a program needn't handle non-finite values.
Results may differ from a plain program's by a relative error of at most 0.007.
Values may be sent and summed in bfloat16 or wider, within the bound.
A program may use at most 128 MiB of HBM per device.

v0:
```python
import jax
import jax.numpy as jnp
from jax import lax
from jax.sharding import PartitionSpec as P


def layer_norm(stream, norm_gain):
    widened = stream.astype(jnp.float32)
    row_mean = jnp.mean(widened, axis=-1, keepdims=True)
    variance = jnp.mean(jnp.square(widened - row_mean), axis=-1, keepdims=True)
    return ((widened - row_mean) * lax.rsqrt(variance + 1e-05) * norm_gain).astype(jnp.bfloat16)


def shared_branch(normed, shared_gate, shared_up, shared_down):
    shared_hidden = (
        jax.nn.silu(jnp.dot(normed, shared_gate, preferred_element_type=jnp.float32))
        * jnp.dot(normed, shared_up, preferred_element_type=jnp.float32)
    ).astype(jnp.bfloat16)
    return jnp.dot(shared_hidden, shared_down, preferred_element_type=jnp.float32)


def serve_rows(received, w_gate, w_up, w_down):
    local_count = w_gate.shape[0]
    blocks = received.reshape((-1, local_count) + received.shape[1:])
    gate_act = jnp.einsum("sxcd,xdh->sxch", blocks, w_gate, preferred_element_type=jnp.float32)
    up_act = jnp.einsum("sxcd,xdh->sxch", blocks, w_up, preferred_element_type=jnp.float32)
    hidden = (jax.nn.silu(gate_act) * up_act).astype(jnp.bfloat16)
    produced = jnp.einsum(
        "sxch,xhd->sxcd", hidden, w_down, preferred_element_type=jnp.float32
    ).astype(jnp.bfloat16)
    return lax.all_to_all(
        produced.reshape(received.shape), "ep", split_axis=0, concat_axis=0, tiled=True
    )


def on_device(
    stream, norm_gain, routing, gates, w_gate, w_up, w_down, shared_gate, shared_up, shared_down
):
    tok_rows, top_count = routing.shape
    local_count = w_gate.shape[0]
    peer_count = lax.axis_size("ep")
    experts = local_count * peer_count
    capacity = 2 * tok_rows * top_count // experts
    normed = layer_norm(stream, norm_gain)
    row_ids = jnp.arange(tok_rows, dtype=jnp.int32)
    lower = (row_ids[:, None] > row_ids[None, :]).astype(jnp.bfloat16)
    slot_ids = jnp.arange(capacity, dtype=jnp.int32).astype(jnp.float32)
    expert_hits = (
        routing[:, :, None] == jnp.arange(experts, dtype=jnp.int32)[None, None, :]
    ).astype(jnp.float32)
    token_hits = jnp.sum(expert_hits, axis=1).astype(jnp.bfloat16)
    earlier = jnp.dot(lower, token_hits, preferred_element_type=jnp.float32)
    slot_index = jnp.sum(earlier[:, None, :] * expert_hits, axis=2)
    slot_hits = (slot_index[:, :, None] == slot_ids[None, None, :]).astype(jnp.float32)
    gate_table = jnp.sum(
        gates[:, :, None, None] * expert_hits[:, :, :, None] * slot_hits[:, :, None, :], axis=1
    )
    all_normed = lax.all_gather(normed, "ep", axis=0, tiled=True)
    all_routing = lax.all_gather(routing, "ep", axis=0, tiled=True)
    first_expert = lax.axis_index("ep") * local_count
    shifted = all_routing.reshape(peer_count, tok_rows, top_count) - first_expert
    local_hits = (
        shifted[:, :, :, None] == jnp.arange(local_count, dtype=jnp.int32)[None, None, None, :]
    ).astype(jnp.float32)
    hits_here = jnp.sum(local_hits, axis=2).astype(jnp.bfloat16)
    prior_here = jnp.einsum("ab,pbx->pax", lower, hits_here, preferred_element_type=jnp.float32)
    placing_here = (
        hits_here.astype(jnp.float32)[:, :, :, None]
        * (prior_here[:, :, :, None] == slot_ids[None, None, None, :]).astype(jnp.float32)
    ).astype(jnp.bfloat16)
    sources = all_normed.reshape(peer_count, tok_rows, all_normed.shape[1])
    incoming = jnp.einsum(
        "ptxc,ptd->pxcd", placing_here, sources, preferred_element_type=jnp.float32
    ).astype(jnp.bfloat16)
    returned = serve_rows(
        incoming.reshape(peer_count * local_count, capacity, all_normed.shape[1]),
        w_gate,
        w_up,
        w_down,
    )
    weight_high = gate_table.astype(jnp.bfloat16)
    weight_low = (gate_table - weight_high.astype(jnp.float32)).astype(jnp.bfloat16)
    routed = jnp.einsum("tec,ecd->td", weight_high, returned, preferred_element_type=jnp.float32)
    routed = routed + jnp.einsum(
        "tec,ecd->td", weight_low, returned, preferred_element_type=jnp.float32
    )
    shared = shared_branch(normed, shared_gate, shared_up, shared_down)
    return (routed + shared).astype(jnp.bfloat16)


def solution(mesh):
    placed = (
        P(("grp", "ep"), None),
        P(),
        P(("grp", "ep"), None),
        P(("grp", "ep"), None),
        P("ep", None, None),
        P("ep", None, None),
        P("ep", None, None),
        P(),
        P(),
        P(),
    )
    return jax.shard_map(
        on_device, mesh=mesh, in_specs=placed, out_specs=P(("grp", "ep"), None), check_vma=False
    )
```

profile of v0, /device:TPU:13, one launch (start us, length us, event | category | flops | bytes accessed | tf_op | source)
XLA Modules:
  0.0 398.3 jit_solution(12400019790795471830)
XLA Ops:
  6.5 1.6 convert_reduce_fusion
  8.2 1.6 fusion.23
  9.8 2.6 fusion.25
  12.4 0.0 all-gather.2.cloned.1.call-update
  12.4 16.1 %all_gather.6 = s32[4096,4]{0,1:T(4,128)S(1)} all-gather(s32[256,4]{0,1:T(4,128)S(1)} %copy-done.3), channel_id=1, replica_groups=mesh['grp'=2,'ep'=16] {'ep'}, dimensions={0}, use_global_device_ids=true | all-gather | bytes 69632 | tf_op jit(solution)/shard_map/all_gather | solution.py:59
  28.6 0.2 convolution_bitcast_fusion.2
  28.8 0.1 copy.22
  28.9 109.1 %all-gather.2.cloned.1.call-done = bf16[4096,2048]{1,0:T(8,128)(2,1)} async-done(((bf16[256,2048]{1,0:T(8,128)(2,1)}), bf16[4096,2048]{1,0:T(8,128)(2,1)}) %all-gather.2.cloned.1.call-update) | async-done | bytes 16777232 | tf_op jit(solution)/shard_map/all_gather | solution.py:58
  137.9 11.5 %convolution_convert_fusion = bf16[16,2,64,2048]{3,2,1,0:T(8,128)(2,1)} fusion(bf16[16,256,2048,1]{2,1,3,0:T(8,128)(2,1)} %bitcast.76, bf16[16,256,2]{1,2,0:T(2,128)(2,1)S(1)} %copy.23, f32[16,256,2]{1,2,0:T(2,128)S(1)} %copy.22, f32[64]{0:T(128)S(1)} %iota_convert_fusion), kind=kOutput, calls=%fused_computation.6 | convolution fusion | flops 2152726528 | bytes 25215232 | tf_op jit(solution)/shard_map/ptxc,ptd->pxcd/dot_general | solution.py:72
  149.5 0.0 copy-done.5
  149.5 9.4 %fusion.2 = f32[2,16,64,512]{3,2,1,0:T(8,128)} fusion(bf16[16,2,64,2048]{3,2,1,0:T(8,128)(2,1)} %convolution_convert_fusion, bf16[2,2048,512]{2,1,0:T(8,128)(2,1)S(1)} %copy-done.5), kind=kOutput, calls=%fused_computation.4 | convolution fusion | flops 4294967296 | bytes 16777216 | tf_op jit(solution)/shard_map/sxcd,xdh->sxch/dot_general | solution.py:25
  158.9 15.3 %convert_bitcast_fusion = bf16[16,2,64,2048]{3,2,0,1:T(8,128)(2,1)} fusion(bf16[2,512,2048]{2,1,0:T(8,128)(2,1)} %param.16, f32[2,16,64,512]{3,2,1,0:T(8,128)} %fusion.2, bf16[2,2048,512]{2,1,0:T(8,128)(2,1)} %param.15, bf16[16,2,64,2048]{3,2,1,0:T(8,128)(2,1)} %convolution_convert_fusion), kind=kOutput, calls=%fused_computation | convolution fusion | flops 8600420352 | bytes 29360128 | tf_op jit(solution)/shard_map/sxch,xhd->sxcd/dot_general | solution.py:28
  174.2 8.3 %copy.26 = bf16[16,2,64,2048]{3,2,1,0:T(8,128)(2,1)} copy(bf16[16,2,64,2048]{3,2,0,1:T(8,128)(2,1)} %convert_bitcast_fusion) | data formatting | bytes 16777216 | tf_op jit(solution)/shard_map/convert_element_type | solution.py:30
  182.4 7.7 %all-to-all-start = ((bf16[32,64,2048]{2,1,0:T(8,128)(2,1)}), bf16[32,64,2048]{2,1,0:T(8,128)(2,1)}, u32[]{:S(2)}, u32[]{:S(2)}) async-start(bf16[32,64,2048]{2,1,0:T(8,128)(2,1)} %bitcast.75), calls=%async_computation | async-start | bytes 16777216 | tf_op jit(solution)/shard_map/all_to_all | solution.py:31
  190.1 0.2 fusion.41
  190.3 0.1 fusion.43
  190.4 0.1 compare_convert_fusion
  190.4 2.0 multiply_reduce_fusion
  192.5 3.1 fusion.49
  195.6 176.9 %all-to-all-done = bf16[32,64,2048]{2,1,0:T(8,128)(2,1)} async-done(((bf16[32,64,2048]{2,1,0:T(8,128)(2,1)}), bf16[32,64,2048]{2,1,0:T(8,128)(2,1)}, u32[]{:S(2)}, u32[]{:S(2)}) %all-to-all-start) | async-done | bytes 8388640 | tf_op jit(solution)/shard_map/all_to_all | solution.py:31
  372.5 7.1 %convolution_bitcast_fusion = f32[256,2048]{1,0:T(8,128)S(1)} fusion(bf16[32,64,2048]{2,1,0:T(8,128)(2,1)} %all-to-all-done, f32[256,32,64]{0,2,1:T(8,128)} %multiply_reduce_fusion), kind=kOutput, calls=%fused_computation.17 | convolution fusion | flops 2149580800 | bytes 12582912 | tf_op jit(solution)/shard_map/tec,ecd->td/dot_general | solution.py:84
  379.6 0.0 copy-done.1
  379.6 7.1 %fusion.11 = f32[256,2048]{1,0:T(8,128)} fusion(f32[256,2048]{1,0:T(8,128)S(1)} %convolution_bitcast_fusion, bf16[32,64,2048]{2,1,0:T(8,128)(2,1)} %all-to-all-done, f32[256,32,64]{0,2,1:T(8,128)S(1)} %copy-done.1), kind=kOutput, calls=%fused_computation.22 | convolution fusion | flops 2148532224 | bytes 14680064 | tf_op jit(solution)/shard_map/tec,ecd->td/dot_general | solution.py:83
  386.8 4.7 %fusion.12 = bf16[256,2048]{1,0:T(8,128)(2,1)} fusion(f32[256,2048]{1,0:T(8,128)} %fusion.11, bf16[512,2048]{1,0:T(8,128)(2,1)S(1)} %copy-done, bf16[256,2048]{1,0:T(8,128)(2,1)S(1)} %copy-done.2, bf16[2048,512]{1,0:T(8,128)(2,1)} %param.18, f32[256,512]{1,0:T(8,128)} %fusion.49), kind=kOutput, calls=%fused_computation.23 | convolution fusion | flops 1075576832 | bytes 8912896 | tf_op jit(solution)/shard_map/dot_general | solution.py:19
  (19 shorter events, 0.1 us)
Async XLA Ops:
  6.5 380.2 %copy-start = (bf16[512,2048]{1,0:T(8,128)(2,1)S(1)}, bf16[512,2048]{1,0:T(8,128)(2,1)}, u32[]{:S(2)}) copy-start(bf16[512,2048]{1,0:T(8,128)(2,1)} %param.19) | copy-start | bytes 6291460
  6.5 5.9 %copy-start.3 = (s32[256,4]{0,1:T(4,128)S(1)}, s32[256,4]{0,1:T(4,128)}, u32[]{:S(2)}) copy-start(s32[256,4]{0,1:T(4,128)} %param.12) | copy-start | bytes 12292
  6.5 131.4 %all-gather.2.cloned.1.call-start = ((), (), s32[]{:S(2)}) async-start(), calls=%async_computation.1 | async-start | bytes 17825792 | tf_op jit(solution)/shard_map/all_gather | solution.py:58
  137.9 11.5 %copy-start.5 = (bf16[2,2048,512]{2,1,0:T(8,128)(2,1)S(1)}, bf16[2,2048,512]{2,1,0:T(8,128)(2,1)}, u32[]{:S(2)}) copy-start(bf16[2,2048,512]{2,1,0:T(8,128)(2,1)} %param.14) | copy-start | bytes 12582916
  182.4 7.9 %copy-start.4 = (f32[256,4]{0,1:T(4,128)S(1)}, f32[256,4]{0,1:T(4,128)}, u32[]{:S(2)}) copy-start(f32[256,4]{0,1:T(4,128)} %param.13) | copy-start | bytes 12292
  182.4 10.0 %copy-start.2 = (bf16[256,2048]{1,0:T(8,128)(2,1)S(1)}, bf16[256,2048]{1,0:T(8,128)(2,1)}, u32[]{:S(2)}) copy-start(bf16[256,2048]{1,0:T(8,128)(2,1)} %fusion.25) | copy-start | bytes 3145732
  182.4 190.0 %all-to-all-start = ((bf16[32,64,2048]{2,1,0:T(8,128)(2,1)}), bf16[32,64,2048]{2,1,0:T(8,128)(2,1)}, u32[]{:S(2)}, u32[]{:S(2)}) async-start(bf16[32,64,2048]{2,1,0:T(8,128)(2,1)} %bitcast.75), calls=%async_computation | async-start | bytes 16777216 | tf_op jit(solution)/shard_map/all_to_all | solution.py:31
  372.5 7.1 %copy-start.1 = (f32[256,32,64]{0,2,1:T(8,128)S(1)}, f32[256,32,64]{0,2,1:T(8,128)}, u32[]{:S(2)}) copy-start(f32[256,32,64]{0,2,1:T(8,128)} %multiply_reduce_fusion) | copy-start | bytes 6291460
Sparse Core Ops, SparseCore 0:
  12.5 125.3 all-gather.1
where the time goes:
time: 399 us; the launch traced here: 398 us
  waiting for transfers between devices  286 us (72%)
  matrix products  58.6 us (15%)
  blocking collectives  16.1 us (4%)
  between operations  13.5 us (3%)
  local copies, waits for them, and re-layouts  8.36 us (2%)
  other arithmetic  8.07 us (2%)
  starting transfers between devices  7.67 us (2%)
    all_to_all x1, waiting for transfers between devices, serve_rows(): lax.all_to_all(produced.reshape(received.shape), 'ep', split_axis=0, conc...  177 us
    all_gather x1, waiting for transfers between devices, on_device(): all_normed = lax.all_gather(normed, 'ep', axis=0, tiled=True)  109 us
    all_gather x1, blocking collectives, on_device(): all_routing = lax.all_gather(routing, 'ep', axis=0, tiled=True)  16.1 us
    dot_general x1, matrix products, serve_rows(): jnp.einsum('sxch,xhd->sxcd', hidden, w_down, preferred_element_type=jnp.f...  15.3 us
    dot_general x1, matrix products, on_device(): jnp.einsum('ptxc,ptd->pxcd', placing_here, sources, preferred_element_typ...  11.5 us
    dot_general x1, matrix products, serve_rows(): jnp.einsum('sxcd,xdh->sxch', blocks, w_gate, preferred_element_type=jnp.f...  9.44 us
    convert_element_type x1, local copies, waits for them, and re-layouts, serve_rows(): produced = jnp.einsum('sxch,xhd->sxcd', hidden, w_down, preferred_element...  8.25 us
  transfers between devices with their start and end apart: 2, of which 2 were waited for; matrix products, arithmetic and copies ran while one was open for 1% of the time, Pallas kernels for 0%

commit v1 on v0

--- a/solution.py
+++ b/solution.py
@@ -1,6 +1,9 @@
+import functools
 import jax
 import jax.numpy as jnp
 from jax import lax
+from jax.experimental import pallas as pl
+from jax.experimental.pallas import tpu as pltpu
 from jax.sharding import PartitionSpec as P
 
 
@@ -33,7 +36,7 @@
     )
 
 
-def on_device(
+def generic_device(
     stream, norm_gain, routing, gates, w_gate, w_up, w_down, shared_gate, shared_up, shared_down
 ):
     tok_rows, top_count = routing.shape
@@ -88,6 +91,381 @@
     return (routed + shared).astype(jnp.bfloat16)
 
 
+OWN, FAR_Y, UP, DOWN, UP_Y, DOWN_Y, OPP, OPP_Y = range(8)
+KEYS = (
+    ["A", "B", "D", "C0", "C1", "E", "F", "G"]
+    + ["S%d" % s for s in range(8)]
+    + ["mA", "mB", "mD", "mC", "mE", "mF", "mG"]
+    + ["mS%d" % s for s in range(8)]
+    + ["P%d" % s for s in range(8)]
+    + ["g", "cA", "cB", "a0", "a1", "b0", "b1", "e", "f", "d"]
+)
+
+
+def fused_kernel(
+    sizes, stream, gain, meta_in, wg_hbm, wu_hbm, wd_hbm, sg_hbm, su_hbm, sd_hbm, out,
+    tok0, tok1, meta, pair_in, full_in, half_in, wg, wu, wd, inc, slot_gate, place, shared,
+    send_sem, recv_sem, load_sem,
+):
+    n, local_count, capacity, top = sizes
+    rows, width = stream.shape
+    half = rows // 2
+    me = lax.axis_index("ep")
+    z, y, core = me // 4, (me // 2) % 2, me % 2
+    depth = n // 4
+
+    def at(zz, yy, cc):
+        return lax.rem(zz, depth) * 4 + yy * 2 + cc
+
+    z_up, z_down = at(z + 1, y, core), at(z + depth - 1, y, core)
+    y_far, sibling = at(z, 1 - y, core), at(z, y, 1 - core)
+
+    barrier = pltpu.get_barrier_semaphore()
+    for peer in (z_up, z_down, y_far, sibling):
+        pl.semaphore_signal(
+            barrier, inc=1, device_id={"ep": peer}, device_id_type=pl.DeviceIdType.MESH
+        )
+
+    loads = [
+        pltpu.make_async_copy(src, dst, load_sem.at[i])
+        for i, (src, dst) in enumerate(
+            [
+                (sg_hbm, wg.at[1]), (su_hbm, wu.at[1]), (sd_hbm, wd.at[1]),
+                (wg_hbm.at[0], wg.at[0]), (wu_hbm.at[0], wu.at[0]), (wd_hbm.at[0], wd.at[0]),
+                (wg_hbm.at[1], wg.at[1]), (wu_hbm.at[1], wu.at[1]), (wd_hbm.at[1], wd.at[1]),
+            ]
+        )
+    ]
+    for load in loads[:6]:
+        load.start()
+
+    low, high = pl.ds(0, half), pl.ds(half, half)
+
+    def own_part(s):
+        return tok0.at[8 + s] if s < 4 else tok0.at[s]
+
+    routes = {
+        "B": (tok0.at[OWN], tok0.at[DOWN], z_up),
+        "A": (tok0.at[OWN], tok0.at[UP], z_down),
+        "D": (tok0.at[OWN], tok0.at[FAR_Y], y_far),
+        "C0": (tok0.at[DOWN, low], tok0.at[OPP, low], z_up),
+        "C1": (tok0.at[UP, high], tok0.at[OPP, high], z_down),
+        "F": (tok0.at[FAR_Y], tok0.at[DOWN_Y], z_up),
+        "E": (tok0.at[FAR_Y], tok0.at[UP_Y], z_down),
+        "G": (tok0.at[OPP], tok0.at[OPP_Y], y_far),
+        "mB": (meta.at[OWN, 0], meta.at[DOWN, 0], z_up),
+        "mA": (meta.at[OWN, 0], meta.at[UP, 0], z_down),
+        "mD": (meta.at[OWN, 0], meta.at[FAR_Y, 0], y_far),
+        "mC": (meta.at[DOWN, 0], meta.at[OPP, 0], z_up),
+        "mF": (meta.at[FAR_Y, 0], meta.at[DOWN_Y, 0], z_up),
+        "mE": (meta.at[FAR_Y, 0], meta.at[UP_Y, 0], z_down),
+        "mG": (meta.at[OPP, 0], meta.at[OPP_Y, 0], y_far),
+        "g": (own_part(OPP_Y), full_in.at[0], y_far),
+        "e": (own_part(UP_Y), full_in.at[1], z_up),
+        "f": (own_part(DOWN_Y), full_in.at[2], z_down),
+        "d": (own_part(FAR_Y), full_in.at[3], y_far),
+        "cA": (own_part(OPP).at[high], half_in.at[0], z_up),
+        "cB": (own_part(OPP).at[low], half_in.at[1], z_down),
+        "a0": (own_part(UP).at[low], full_in.at[4, low], z_up),
+        "a1": (own_part(UP).at[high], full_in.at[4, high], z_up),
+        "b0": (own_part(DOWN).at[low], full_in.at[5, low], z_down),
+        "b1": (own_part(DOWN).at[high], full_in.at[5, high], z_down),
+    }
+    for s in range(8):
+        routes["S%d" % s] = (tok0.at[s], tok1.at[s], sibling)
+        routes["mS%d" % s] = (meta.at[s, 0], meta.at[s, 1], sibling)
+        routes["P%d" % s] = (tok1.at[s], pair_in.at[s], sibling)
+
+    def copy_of(key):
+        src, dst, peer = routes[key]
+        i = KEYS.index(key)
+        return pltpu.make_async_remote_copy(
+            src_ref=src, dst_ref=dst, send_sem=send_sem.at[i], recv_sem=recv_sem.at[i],
+            device_id={"ep": peer}, device_id_type=pl.DeviceIdType.MESH,
+        )
+
+    def send(*keys):
+        for key in keys:
+            copy_of(key).start()
+
+    def arrived(*keys):
+        for key in keys:
+            copy_of(key).wait_recv()
+
+    def sent(*keys):
+        for key in keys:
+            copy_of(key).wait_send()
+
+    piece = 32
+
+    def norm_rows(i, carry):
+        span = pl.ds(pl.multiple_of(i * piece, piece), piece)
+        wide = stream[span, :].astype(jnp.float32)
+        mean = jnp.mean(wide, axis=-1, keepdims=True)
+        centred = wide - mean
+        var = jnp.mean(centred * centred, axis=-1, keepdims=True)
+        tok0[OWN, span, :] = (centred * lax.rsqrt(var + 1e-05) * gain[...]).astype(jnp.bfloat16)
+        return carry
+
+    lax.fori_loop(0, rows // piece, norm_rows, 0)
+    meta[OWN, 0] = meta_in[...]
+    pl.semaphore_wait(barrier, 4)
+    send("mB", "mA", "mD", "mS0", "B", "A", "D", "S0")
+
+    def hidden_of(x, slot):
+        gate = jnp.dot(x, wg[slot], preferred_element_type=jnp.float32)
+        up = jnp.dot(x, wu[slot], preferred_element_type=jnp.float32)
+        return jax.nn.silu(gate) * up
+
+    cols = width // 4
+
+    for load in loads[:3]:
+        load.wait()
+    hidden = hidden_of(tok0[OWN], 1).astype(jnp.bfloat16)
+    for c in range(4):
+        part = pl.ds(c * cols, cols)
+        shared[:, part] = jnp.dot(hidden, wd[1, :, part], preferred_element_type=jnp.float32)
+    for load in loads[6:]:
+        load.start()
+
+    first = (me * local_count).astype(jnp.float32)
+    tri = (
+        lax.broadcasted_iota(jnp.int32, (rows, rows), 0)
+        < lax.broadcasted_iota(jnp.int32, (rows, rows), 1)
+    ).astype(jnp.float32).astype(jnp.bfloat16)
+    slots = local_count * capacity
+    slot_row = lax.broadcasted_iota(jnp.int32, (slots, rows), 0).astype(jnp.float32)
+    stack_row = lax.broadcasted_iota(jnp.int32, (8, rows), 0)
+
+    def serve_group(base):
+        stacked = jnp.zeros((8, rows), jnp.float32)
+        gate_rows, hit_rows = [], []
+        for k in range(4):
+            m = meta[base + k // 2, k % 2]
+            ids, weights = m[0:top], m[top:2 * top]
+            for x in range(local_count):
+                match = (ids == first + x).astype(jnp.float32)
+                hit = jnp.sum(match, axis=0, keepdims=True)
+                hit_rows.append(hit)
+                gate_rows.append(jnp.sum(match * weights, axis=0, keepdims=True))
+                stacked = jnp.where(stack_row == k * local_count + x, hit, stacked)
+        prior = jnp.dot(stacked.astype(jnp.bfloat16), tri, preferred_element_type=jnp.float32)
+        for k in range(4):
+            j, r = k // 2, k % 2
+            chosen = jnp.zeros((slots, rows), jnp.float32)
+            weighted = jnp.zeros((slots, rows), jnp.float32)
+            for x in range(local_count):
+                q = k * local_count + x
+                row = jnp.where(hit_rows[q] > 0, prior[q:q + 1] + x * capacity, -1.0)
+                same = (slot_row == row).astype(jnp.float32)
+                chosen = chosen + same
+                weighted = weighted + same * gate_rows[q]
+            slot_gate[k] = jnp.broadcast_to(jnp.sum(weighted, axis=1, keepdims=True), (slots, 128))
+            place[k] = chosen.astype(jnp.bfloat16)
+            source = tok0 if r == 0 else tok1
+            for c in range(4):
+                part = pl.ds(c * cols, cols)
+                inc[k, :, part] = jnp.dot(
+                    place[k], source[base + j, :, part], preferred_element_type=jnp.float32
+                ).astype(jnp.bfloat16)
+        for x in range(local_count):
+            mine = pl.ds(x * capacity, capacity)
+            taken = inc[:, mine, :].reshape(4 * capacity, width)
+            scale = slot_gate[:, mine, :].reshape(4 * capacity, 128)[:, 0:1]
+            act = (hidden_of(taken, x) * scale).astype(jnp.bfloat16)
+            for c in range(4):
+                part = pl.ds(c * cols, cols)
+                made = jnp.dot(act, wd[x, :, part], preferred_element_type=jnp.float32)
+                inc[:, mine, part] = made.astype(jnp.bfloat16).reshape(4, capacity, cols)
+
+    def combine_group(base, g):
+        for k in range(4):
+            j, r = k // 2, k % 2
+            for c in range(4):
+                part = pl.ds(c * cols, cols)
+                total = lax.dot_general(
+                    place[k], inc[k, :, part], (((0,), (0,)), ((), ())),
+                    preferred_element_type=jnp.float32,
+                ).astype(jnp.bfloat16)
+                if r == 0:
+                    tok0[base + j + 8 * (1 - g // 2), :, part] = total
+                else:
+                    tok1[base + j, :, part] = total
+
+    def add_into(dst, others, begin, count):
+        def step(i, carry):
+            span = pl.ds(pl.multiple_of(begin + i * piece, piece), piece)
+            total = dst[span, :].astype(jnp.float32)
+            for other, offset in others:
+                there = pl.ds(pl.multiple_of(begin - offset + i * piece, piece), piece)
+                total = total + other[there, :].astype(jnp.float32)
+            dst[span, :] = total.astype(jnp.bfloat16)
+            return carry
+
+        lax.fori_loop(0, count // piece, step, 0)
+
+    def group(g, carry):
+        @pl.when(g == 0)
+        def _():
+            arrived("mB", "mA", "mD", "mS0")
+            send("mC", "mF", "mE", "mS1", "mS2", "mS3")
+            arrived("B")
+            send("C0", "S3")
+            arrived("A")
+            send("C1", "S2")
+            arrived("D")
+            send("F", "E", "S1")
+            arrived("mC")
+            send("mG", "mS6")
+            arrived("mE", "mF")
+            send("mS4", "mS5")
+            for load in loads[3:]:
+                load.wait()
+            arrived("S0", "S1", "mS1")
+
+        @pl.when(g == 1)
+        def _():
+            arrived("S2", "S3", "mS2", "mS3")
+
+        @pl.when(g == 2)
+        def _():
+            arrived("C0", "C1")
+            send("G", "S6")
+            arrived("E")
+            send("S4")
+            arrived("F")
+            send("S5")
+            arrived("S4", "S5", "mS4", "mS5")
+
+        @pl.when(g == 3)
+        def _():
+            arrived("mG", "G")
+            send("mS7", "S7")
+            arrived("mS6", "S6", "mS7", "S7")
+
+        base = 2 * g
+        serve_group(base)
+
+        @pl.when(g == 2)
+        def _():
+            sent("S4", "S5")
+
+        @pl.when(g == 3)
+        def _():
+            sent("S6", "G", "S7")
+
+        combine_group(base, g)
+
+        @pl.when(g == 0)
+        def _():
+            send("P0", "P1")
+
+        @pl.when(g == 1)
+        def _():
+            send("P2", "P3")
+
+        @pl.when(g == 2)
+        def _():
+            send("P4", "P5")
+            arrived("P4")
+            add_into(own_part(UP_Y), [(pair_in.at[UP_Y], 0)], 0, rows)
+            send("e")
+            arrived("P5")
+            add_into(own_part(DOWN_Y), [(pair_in.at[DOWN_Y], 0)], 0, rows)
+            send("f")
+
+        @pl.when(g == 3)
+        def _():
+            send("P7", "P6")
+
+        return carry
+
+    lax.fori_loop(0, 4, group, 0)
+    arrived("P7")
+    add_into(own_part(OPP_Y), [(pair_in.at[OPP_Y], 0)], 0, rows)
+    send("g")
+    arrived("P2", "P3")
+    add_into(own_part(UP), [(pair_in.at[UP], 0)], 0, half)
+    send("a0")
+    add_into(own_part(DOWN), [(pair_in.at[DOWN], 0)], half, half)
+    send("b1")
+    arrived("P0", "P1", "P6", "e", "f")
+    add_into(
+        own_part(FAR_Y), [(pair_in.at[FAR_Y], 0), (full_in.at[1], 0), (full_in.at[2], 0)], 0, rows
+    )
+    send("d")
+    arrived("g")
+    add_into(own_part(OPP), [(pair_in.at[OPP], 0), (full_in.at[0], 0)], 0, rows)
+    send("cA", "cB")
+    arrived("cA")
+    add_into(own_part(UP), [(pair_in.at[UP], 0), (half_in.at[0], half)], half, half)
+    send("a1")
+    arrived("cB")
+    add_into(own_part(DOWN), [(pair_in.at[DOWN], 0), (half_in.at[1], 0)], 0, half)
+    send("b0")
+    arrived("a0", "b1", "d", "a1", "b0")
+
+    def finish(i, carry):
+        span = pl.ds(pl.multiple_of(i * piece, piece), piece)
+        total = shared[span, :] + tok0[8 + OWN, span, :].astype(jnp.float32)
+        for other in (pair_in.at[OWN], full_in.at[3], full_in.at[4], full_in.at[5]):
+            total = total + other[span, :].astype(jnp.float32)
+        out[span, :] = total.astype(jnp.bfloat16)
+        return carry
+
+    lax.fori_loop(0, rows // piece, finish, 0)
+    waited = ("S4", "S5", "S6", "G", "S7")
+    sent(*[key for key in KEYS if key not in waited])
+
+
+def fused_device(
+    stream, norm_gain, routing, gates, w_gate, w_up, w_down, shared_gate, shared_up, shared_down
+):
+    rows, width = stream.shape
+    top = routing.shape[1]
+    local_count, _, hidden = w_gate.shape
+    n = lax.axis_size("ep")
+    capacity = 2 * rows * top // (local_count * n)
+    slots = local_count * capacity
+    meta = jnp.concatenate([routing.astype(jnp.float32), gates], axis=1).T
+    bf16, f32 = jnp.bfloat16, jnp.float32
+    vmem, anywhere = pl.BlockSpec(memory_space=pltpu.VMEM), pl.BlockSpec(memory_space=pl.ANY)
+    return pl.pallas_call(
+        functools.partial(fused_kernel, (n, local_count, capacity, top)),
+        out_shape=jax.ShapeDtypeStruct((rows, width), bf16),
+        in_specs=[vmem] * 3 + [anywhere] * 6,
+        out_specs=vmem,
+        scratch_shapes=[
+            pltpu.VMEM((12, rows, width), bf16),
+            pltpu.VMEM((8, rows, width), bf16),
+            pltpu.VMEM((8, 2, 2 * top, rows), f32),
+            pltpu.VMEM((8, rows, width), bf16),
+            pltpu.VMEM((6, rows, width), bf16),
+            pltpu.VMEM((2, rows // 2, width), bf16),
+            pltpu.VMEM((2, width, hidden), bf16),
+            pltpu.VMEM((2, width, hidden), bf16),
+            pltpu.VMEM((2, hidden, width), bf16),
+            pltpu.VMEM((4, slots, width), bf16),
+            pltpu.VMEM((4, slots, 128), f32),
+            pltpu.VMEM((4, slots, rows), bf16),
+            pltpu.VMEM((rows, width), f32),
+            pltpu.SemaphoreType.DMA((len(KEYS),)),
+            pltpu.SemaphoreType.DMA((len(KEYS),)),
+            pltpu.SemaphoreType.DMA((9,)),
+        ],
+        compiler_params=pltpu.CompilerParams(
+            collective_id=0, has_side_effects=True, vmem_limit_bytes=63 * 1024 * 1024
+        ),
+    )(stream, norm_gain.reshape(1, -1), meta, w_gate, w_up, w_down, shared_gate, shared_up, shared_down)
+
+
+def on_device(stream, norm_gain, routing, gates, w_gate, *rest):
+    ring = lax.axis_size("ep") // 4
+    fits = ring == 4 and w_gate.shape[0] == 2 and rest[2].shape == w_gate.shape[1:]
+    run = fused_device if fits else generic_device
+    return run(stream, norm_gain, routing, gates, w_gate, *rest)
+
+
 def solution(mesh):
     placed = (
         P(("grp", "ep"), None),

time: 399 us -> 256 us (0.64)
  the two profiles are of different devices: /device:TPU:13 before, /device:TPU:0 now
where the time goes in v1:
time: 256 us
  Pallas kernels  251 us (98%)
    pallas_call x1, Pallas kernels, fused_device(): pl.pallas_call(functools.partial(fused_kernel, (n, local_count, capacity,...  251 us

profile of v1, /device:TPU:0, one launch (start us, length us, event | category | flops | bytes accessed | tf_op | source)
XLA Modules:
  0.0 255.6 jit_solution(5581567737939738251)
XLA Ops:
  0.0 0.7 convert_element_type.3
  0.7 1.3 maximum_bitcast_fusion.meta_in
  2.0 251.3 %shard_map.100 = bf16[256,2048]{1,0:T(8,128)(2,1)} custom-call(bf16[256,2048]{1,0:T(8,128)(2,1)} %stream.1, f32[1,2048]{1,0:T(1,128)} %bitcast.3, f32[8,256]{1,0:T(8,128)} %maximum_bitcast_fusion.meta_in, bf16[2,2048,512]{2,1,0:T(8,128)(2,1)} %wg_hbm.1, bf16[2,2048,512]{2,1,0:T(8,128)(2,1)} %wu_hbm.1, bf16[2,512,2048]{2,1,0:T(8,128)(2,1)} %wd_hbm.1, ...), custom_call_target="tpu_custom_call" | custom-call | tf_op jit(solution)/shard_map/pallas_call | solution.py:433
  253.3 2.3 copy.12

commit v2 on v1

--- a/solution.py
+++ b/solution.py
@@ -91,37 +91,46 @@
     return (routed + shared).astype(jnp.bfloat16)
 
 
-OWN, FAR_Y, UP, DOWN, UP_Y, DOWN_Y, OPP, OPP_Y = range(8)
+PLACE = {1: 0, 7: 1, 2: 2, 6: 3, 3: 4, 5: 5, 0: 6, 4: 7}
+OWN = PLACE[0]
 KEYS = (
-    ["A", "B", "D", "C0", "C1", "E", "F", "G"]
-    + ["S%d" % s for s in range(8)]
-    + ["mA", "mB", "mD", "mC", "mE", "mF", "mG"]
-    + ["mS%d" % s for s in range(8)]
-    + ["P%d" % s for s in range(8)]
-    + ["g", "cA", "cB", "a0", "a1", "b0", "b1", "e", "f", "d"]
+    ["M4", "N4"]
+    + [way + str(k) + part for way, first in (("M", 1), ("N", 5)) for k in range(first, first + 3)
+       for part in ("l", "h")]
+    + ["mM1", "mM2", "mM3", "mM4", "mN7", "mN6", "mN5"]
+    + ["S%d" % k for k in range(8)]
+    + ["mS%d" % k for k in range(8)]
+    + ["P%d" % k for k in range(8)]
+    + ["u4", "d4"]
+    + [way + str(k) + part for way, first in (("u", 1), ("d", 5)) for k in range(first, first + 3)
+       for part in ("l", "h")]
 )
 
 
 def fused_kernel(
     sizes, stream, gain, meta_in, wg_hbm, wu_hbm, wd_hbm, sg_hbm, su_hbm, sd_hbm, out,
-    tok0, tok1, meta, pair_in, full_in, half_in, wg, wu, wd, inc, slot_gate, place, shared,
+    tok0, tok1, meta, pair_in, flow_in, wg, wu, wd, inc, slot_gate, place, shared,
     send_sem, recv_sem, load_sem,
 ):
     n, local_count, capacity, top = sizes
     rows, width = stream.shape
     half = rows // 2
     me = lax.axis_index("ep")
+    depth = n // 4
+    chips = 2 * depth
     z, y, core = me // 4, (me // 2) % 2, me % 2
-    depth = n // 4
-
-    def at(zz, yy, cc):
-        return lax.rem(zz, depth) * 4 + yy * 2 + cc
-
-    z_up, z_down = at(z + 1, y, core), at(z + depth - 1, y, core)
-    y_far, sibling = at(z, 1 - y, core), at(z, y, 1 - core)
+    spot = z + y * (chips - 1 - 2 * z)
+
+    def at(where, cc):
+        where = lax.rem(where, chips)
+        yy = where // depth
+        zz = where + yy * (chips - 1 - 2 * where)
+        return zz * 4 + yy * 2 + cc
+
+    up, down, sibling = at(spot + 1, core), at(spot + chips - 1, core), at(spot, 1 - core)
 
     barrier = pltpu.get_barrier_semaphore()
-    for peer in (z_up, z_down, y_far, sibling):
+    for peer in (up, down, sibling):
         pl.semaphore_signal(
             barrier, inc=1, device_id={"ep": peer}, device_id_type=pl.DeviceIdType.MESH
         )
@@ -141,40 +150,37 @@
 
     low, high = pl.ds(0, half), pl.ds(half, half)
 
-    def own_part(s):
-        return tok0.at[8 + s] if s < 4 else tok0.at[s]
+    def tok(k):
+        return tok0.at[PLACE[k]]
+
+    def own_part(k):
+        return tok0.at[PLACE[k] + (8 if PLACE[k] < 6 else 0)]
 
     routes = {
-        "B": (tok0.at[OWN], tok0.at[DOWN], z_up),
-        "A": (tok0.at[OWN], tok0.at[UP], z_down),
-        "D": (tok0.at[OWN], tok0.at[FAR_Y], y_far),
-        "C0": (tok0.at[DOWN, low], tok0.at[OPP, low], z_up),
-        "C1": (tok0.at[UP, high], tok0.at[OPP, high], z_down),
-        "F": (tok0.at[FAR_Y], tok0.at[DOWN_Y], z_up),
-        "E": (tok0.at[FAR_Y], tok0.at[UP_Y], z_down),
-        "G": (tok0.at[OPP], tok0.at[OPP_Y], y_far),
-        "mB": (meta.at[OWN, 0], meta.at[DOWN, 0], z_up),
-        "mA": (meta.at[OWN, 0], meta.at[UP, 0], z_down),
-        "mD": (meta.at[OWN, 0], meta.at[FAR_Y, 0], y_far),
-        "mC": (meta.at[DOWN, 0], meta.at[OPP, 0], z_up),
-        "mF": (meta.at[FAR_Y, 0], meta.at[DOWN_Y, 0], z_up),
-        "mE": (meta.at[FAR_Y, 0], meta.at[UP_Y, 0], z_down),
-        "mG": (meta.at[OPP, 0], meta.at[OPP_Y, 0], y_far),
-        "g": (own_part(OPP_Y), full_in.at[0], y_far),
-        "e": (own_part(UP_Y), full_in.at[1], z_up),
-        "f": (own_part(DOWN_Y), full_in.at[2], z_down),
-        "d": (own_part(FAR_Y), full_in.at[3], y_far),
-        "cA": (own_part(OPP).at[high], half_in.at[0], z_up),
-        "cB": (own_part(OPP).at[low], half_in.at[1], z_down),
-        "a0": (own_part(UP).at[low], full_in.at[4, low], z_up),
-        "a1": (own_part(UP).at[high], full_in.at[4, high], z_up),
-        "b0": (own_part(DOWN).at[low], full_in.at[5, low], z_down),
-        "b1": (own_part(DOWN).at[high], full_in.at[5, high], z_down),
+        "M4": (tok(3).at[low], tok(4).at[low], down),
+        "N4": (tok(5).at[high], tok(4).at[high], up),
+        "mM4": (meta.at[PLACE[3], 0], meta.at[PLACE[4], 0], down),
+        "u4": (own_part(4).at[high], flow_in.at[3, high], up),
+        "d4": (own_part(4).at[low], flow_in.at[4, low], down),
     }
-    for s in range(8):
-        routes["S%d" % s] = (tok0.at[s], tok1.at[s], sibling)
-        routes["mS%d" % s] = (meta.at[s, 0], meta.at[s, 1], sibling)
-        routes["P%d" % s] = (tok1.at[s], pair_in.at[s], sibling)
+    for k in (1, 2, 3):
+        routes["mM%d" % k] = (meta.at[PLACE[k - 1], 0], meta.at[PLACE[k], 0], down)
+        behind = (9 - k) % 8
+        routes["mN%d" % (8 - k)] = (meta.at[PLACE[behind], 0], meta.at[PLACE[8 - k], 0], up)
+        for name, rows_of in (("l", low), ("h", high)):
+            routes["M%d%s" % (k, name)] = (tok(k - 1).at[rows_of], tok(k).at[rows_of], down)
+            routes["N%d%s" % (8 - k, name)] = (tok(behind).at[rows_of], tok(8 - k).at[rows_of], up)
+            routes["u%d%s" % (k, name)] = (
+                own_part(k).at[rows_of], flow_in.at[k - 1, rows_of], up
+            )
+            routes["d%d%s" % (8 - k, name)] = (
+                own_part(8 - k).at[rows_of], flow_in.at[8 - k, rows_of], down
+            )
+    for k in range(8):
+        s = PLACE[k]
+        routes["S%d" % k] = (tok0.at[s], tok1.at[s], sibling)
+        routes["mS%d" % k] = (meta.at[s, 0], meta.at[s, 1], sibling)
+        routes["P%d" % k] = (tok1.at[s], pair_in.at[s], sibling)
 
     def copy_of(key):
         src, dst, peer = routes[key]
@@ -209,8 +215,8 @@
 
     lax.fori_loop(0, rows // piece, norm_rows, 0)
     meta[OWN, 0] = meta_in[...]
-    pl.semaphore_wait(barrier, 4)
-    send("mB", "mA", "mD", "mS0", "B", "A", "D", "S0")
+    pl.semaphore_wait(barrier, 3)
+    send("mM1", "mN7", "mS0", "M1l", "N7h", "M1h", "N7l", "S0")
 
     def hidden_of(x, slot):
         gate = jnp.dot(x, wg[slot], preferred_element_type=jnp.float32)
@@ -288,7 +294,7 @@
                     preferred_element_type=jnp.float32,
                 ).astype(jnp.bfloat16)
                 if r == 0:
-                    tok0[base + j + 8 * (1 - g // 2), :, part] = total
+                    tok0[base + j + 8 * (1 - g // 3), :, part] = total
                 else:
                     tok1[base + j, :, part] = total
 
@@ -304,117 +310,126 @@
 
         lax.fori_loop(0, count // piece, step, 0)
 
+    def pair(k):
+        return (pair_in.at[PLACE[k]], 0)
+
     def group(g, carry):
         @pl.when(g == 0)
         def _():
-            arrived("mB", "mA", "mD", "mS0")
-            send("mC", "mF", "mE", "mS1", "mS2", "mS3")
-            arrived("B")
-            send("C0", "S3")
-            arrived("A")
-            send("C1", "S2")
-            arrived("D")
-            send("F", "E", "S1")
-            arrived("mC")
-            send("mG", "mS6")
-            arrived("mE", "mF")
-            send("mS4", "mS5")
+            arrived("mM1", "mN7")
+            send("mM2", "mN6", "mS1", "mS7")
+            arrived("M1l")
+            send("M2l")
+            arrived("N7h")
+            send("N6h")
+            arrived("M1h")
+            send("M2h")
+            arrived("N7l")
+            send("N6l", "S1", "S7")
             for load in loads[3:]:
                 load.wait()
-            arrived("S0", "S1", "mS1")
+            arrived("S1", "S7", "mS1", "mS7")
 
         @pl.when(g == 1)
         def _():
-            arrived("S2", "S3", "mS2", "mS3")
+            arrived("mM2", "mN6")
+            send("mM3", "mN5", "mS2", "mS6")
+            arrived("M2l")
+            send("M3l")
+            arrived("N6h")
+            send("N5h")
+            arrived("M2h")
+            send("M3h")
+            arrived("N6l")
+            send("N5l", "S2", "S6")
+            arrived("S2", "S6", "mS2", "mS6")
 
         @pl.when(g == 2)
         def _():
-            arrived("C0", "C1")
-            send("G", "S6")
-            arrived("E")
-            send("S4")
-            arrived("F")
-            send("S5")
-            arrived("S4", "S5", "mS4", "mS5")
+            arrived("mM3", "mN5")
+            send("mM4", "mS3", "mS5")
+            arrived("M3l")
+            send("M4")
+            arrived("N5h")
+            send("N4")
+            arrived("M3h", "N5l")
+            send("S3", "S5")
+            arrived("S3", "S5", "mS3", "mS5")
 
         @pl.when(g == 3)
         def _():
-            arrived("mG", "G")
-            send("mS7", "S7")
-            arrived("mS6", "S6", "mS7", "S7")
+            arrived("mM4", "M4", "N4")
+            send("mS4", "S4")
+            arrived("S0", "mS0", "S4", "mS4")
 
         base = 2 * g
         serve_group(base)
 
+        @pl.when(g == 3)
+        def _():
+            sent("S0", "S4", "M1l", "M1h", "N7l", "N7h")
+
+        combine_group(base, g)
+
+        @pl.when(g == 0)
+        def _():
+            send("P1", "P7")
+
+        @pl.when(g == 1)
+        def _():
+            send("P2", "P6")
+
         @pl.when(g == 2)
         def _():
-            sent("S4", "S5")
+            send("P3", "P5")
+            arrived("P3")
+            add_into(own_part(3), [pair(3)], 0, half)
+            send("u3l")
+            arrived("P5")
+            add_into(own_part(5), [pair(5)], half, half)
+            send("d5h")
 
         @pl.when(g == 3)
         def _():
-            sent("S6", "G", "S7")
-
-        combine_group(base, g)
-
-        @pl.when(g == 0)
-        def _():
-            send("P0", "P1")
-
-        @pl.when(g == 1)
-        def _():
-            send("P2", "P3")
-
-        @pl.when(g == 2)
-        def _():
-            send("P4", "P5")
-            arrived("P4")
-            add_into(own_part(UP_Y), [(pair_in.at[UP_Y], 0)], 0, rows)
-            send("e")
-            arrived("P5")
-            add_into(own_part(DOWN_Y), [(pair_in.at[DOWN_Y], 0)], 0, rows)
-            send("f")
-
-        @pl.when(g == 3)
-        def _():
-            send("P7", "P6")
+            send("P4", "P0")
 
         return carry
 
     lax.fori_loop(0, 4, group, 0)
-    arrived("P7")
-    add_into(own_part(OPP_Y), [(pair_in.at[OPP_Y], 0)], 0, rows)
-    send("g")
-    arrived("P2", "P3")
-    add_into(own_part(UP), [(pair_in.at[UP], 0)], 0, half)
-    send("a0")
-    add_into(own_part(DOWN), [(pair_in.at[DOWN], 0)], half, half)
-    send("b1")
-    arrived("P0", "P1", "P6", "e", "f")
-    add_into(
-        own_part(FAR_Y), [(pair_in.at[FAR_Y], 0), (full_in.at[1], 0), (full_in.at[2], 0)], 0, rows
-    )
-    send("d")
-    arrived("g")
-    add_into(own_part(OPP), [(pair_in.at[OPP], 0), (full_in.at[0], 0)], 0, rows)
-    send("cA", "cB")
-    arrived("cA")
-    add_into(own_part(UP), [(pair_in.at[UP], 0), (half_in.at[0], half)], half, half)
-    send("a1")
-    arrived("cB")
-    add_into(own_part(DOWN), [(pair_in.at[DOWN], 0), (half_in.at[1], 0)], 0, half)
-    send("b0")
-    arrived("a0", "b1", "d", "a1", "b0")
+    arrived("P4")
+    add_into(own_part(4), [pair(4)], half, half)
+    send("u4")
+    add_into(own_part(4), [pair(4)], 0, half)
+    send("d4")
+    arrived("P0", "P1", "P2", "P6", "P7")
+
+    def pass_on(key, dst, k, landing, begin):
+        arrived(key)
+        add_into(dst, [pair(k), (flow_in.at[landing], 0)], begin, half)
+
+    pass_on("u4", own_part(3), 3, 3, half)
+    send("u3h")
+    pass_on("d4", own_part(5), 5, 4, 0)
+    send("d5l")
+    for k in (2, 1):
+        for name, begin in (("l", 0), ("h", half)):
+            other = "h" if name == "l" else "l"
+            pass_on("u%d%s" % (k + 1, name), own_part(k), k, k, begin)
+            send("u%d%s" % (k, name))
+            pass_on("d%d%s" % (7 - k, other), own_part(8 - k), 8 - k, 7 - k, half - begin)
+            send("d%d%s" % (8 - k, other))
+    arrived("u1l", "u1h", "d7l", "d7h")
 
     def finish(i, carry):
         span = pl.ds(pl.multiple_of(i * piece, piece), piece)
-        total = shared[span, :] + tok0[8 + OWN, span, :].astype(jnp.float32)
-        for other in (pair_in.at[OWN], full_in.at[3], full_in.at[4], full_in.at[5]):
+        total = shared[span, :] + tok0[OWN, span, :].astype(jnp.float32)
+        for other in (pair_in.at[OWN], flow_in.at[0], flow_in.at[7]):
             total = total + other[span, :].astype(jnp.float32)
         out[span, :] = total.astype(jnp.bfloat16)
         return carry
 
     lax.fori_loop(0, rows // piece, finish, 0)
-    waited = ("S4", "S5", "S6", "G", "S7")
+    waited = ("S0", "S4", "M1l", "M1h", "N7l", "N7h")
     sent(*[key for key in KEYS if key not in waited])
 
 
@@ -436,12 +451,11 @@
         in_specs=[vmem] * 3 + [anywhere] * 6,
         out_specs=vmem,
         scratch_shapes=[
-            pltpu.VMEM((12, rows, width), bf16),
+            pltpu.VMEM((14, rows, width), bf16),
             pltpu.VMEM((8, rows, width), bf16),
             pltpu.VMEM((8, 2, 2 * top, rows), f32),
             pltpu.VMEM((8, rows, width), bf16),
-            pltpu.VMEM((6, rows, width), bf16),
-            pltpu.VMEM((2, rows // 2, width), bf16),
+            pltpu.VMEM((8, rows, width), bf16),
             pltpu.VMEM((2, width, hidden), bf16),
             pltpu.VMEM((2, width, hidden), bf16),
             pltpu.VMEM((2, hidden, width), bf16),

time: 256 us -> 178 us (0.70)
  Pallas kernels: 251 us -> 173 us
    pallas_call x1, Pallas kernels: 251 us -> 173 us  [fused_device(): pl.pallas_call(functools.partial(fused_kernel, (n, local_count, capacity,...]
where the time goes in v2:
time: 178 us; the launch traced here: 177 us
  Pallas kernels  173 us (97%)
  local copies, waits for them, and re-layouts  2.3 us (1%)
  other arithmetic  1.98 us (1%)
    pallas_call x1, Pallas kernels, fused_device(): pl.pallas_call(functools.partial(fused_kernel, (n, local_count, capacity,...  173 us

profile of v2, /device:TPU:0, one launch (start us, length us, event | category | flops | bytes accessed | tf_op | source)
XLA Modules:
  0.0 177.3 jit_solution(10561745799029415599)
XLA Ops:
  0.0 0.7 convert_element_type.3
  0.7 1.3 maximum_bitcast_fusion.meta_in
  2.0 173.0 %shard_map.100 = bf16[256,2048]{1,0:T(8,128)(2,1)} custom-call(bf16[256,2048]{1,0:T(8,128)(2,1)} %stream.1, f32[1,2048]{1,0:T(1,128)} %bitcast.3, f32[8,256]{1,0:T(8,128)} %maximum_bitcast_fusion.meta_in, bf16[2,2048,512]{2,1,0:T(8,128)(2,1)} %wg_hbm.1, bf16[2,2048,512]{2,1,0:T(8,128)(2,1)} %wu_hbm.1, bf16[2,512,2048]{2,1,0:T(8,128)(2,1)} %wd_hbm.1, ...), custom_call_target="tpu_custom_call" | custom-call | tf_op jit(solution)/shard_map/pallas_call | solution.py:448
  175.0 2.3 %copy.12 = bf16[256,2048]{1,0:T(8,128)(2,1)} copy(bf16[256,2048]{1,0:T(8,128)(2,1)} %shard_map.100) | data formatting | bytes 2097152
